TPU v7x, 32 devices: a whole 2x2x4 slice. The times are simulated.
32 devices in a mesh: sp: 8 (over z, y), tp: 4 (over x, core).
Axes of the slice: x: 2, y: 2, z: 4, core: 2. Of those that a mesh axis runs over, the one named last changes fastest.
Arguments:
- queries: bfloat16 [2304, 2048], P('sp', 'tp'), as said below
- key_vectors: bfloat16 [2304, 2048], P('sp', 'tp'), as said below
- latents: bfloat16 [2304, 2048], P('sp'), as said below
- value_weight: bfloat16 [2048, 2048], P(None, 'tp'), as said below
- log_sums: float32 [2304, 32], P('sp', 'tp'), as said below
- out_first: bfloat16 [2304, 2048], P('sp', 'tp'), as said below
- out_second: bfloat16 [2304, 2048], P('sp', 'tp'), as said below
- cotangent: bfloat16 [2304, 2048], P('sp', 'tp'), may hold values from -6 to 6
- head_lambda: float32 [16], P('tp'), may hold values from 0.3 to 0.8
Outputs:
- grad_queries: float32 [2304, 2048], P('sp', 'tp')
- grad_keys: float32 [2304, 2048], P('sp', 'tp')
- grad_latents: bfloat16 [2304, 2048], P('sp', 'tp')
- grad_weight: float32 [2048, 2048], P('sp', 'tp')
Inputs may be any that keep to these rules, and one draw needn't show every extreme that they name: queries with entries of standard deviation 1.75. `key_vectors`: keys with entries of standard deviation 1. `latents`: inputs of standard deviation 1. `value_weight`: weights scaled by the inverse square root of 2048. `log_sums`: each row's log-sum of exponentials of its causal scores, for the given queries and keys. `out_first`: the first map's attention output for the given queries, keys, values and log-sums. `out_second`: the second map's attention output, likewise.
All inputs are finite; a program needn't handle non-finite values.
Results may differ from a plain program's by a relative error of at most 0.022.
Values may be sent and summed in bfloat16 or wider, within the bound.
A program may use at most 192 MiB of HBM per device.

v0:
```python
import jax
import jax.numpy as jnp
from jax import lax
from jax.sharding import PartitionSpec as P

DH = 64
DV = 128


def row_terms(out_first, out_second, cotangent, head_lambda):
    count = out_first.shape[0]
    head_count = head_lambda.shape[0]
    first = out_first.astype(jnp.float32).reshape(count, head_count, DV)
    second = out_second.astype(jnp.float32).reshape(count, head_count, DV)
    mixed = first - head_lambda[None, :, None] * second
    inverse = lax.rsqrt(jnp.mean(mixed * mixed, axis=-1, keepdims=True) + 1e-06)
    normed = mixed * inverse
    grad_out = cotangent.astype(jnp.float32).reshape(count, head_count, DV)
    grad_mixed = inverse * (grad_out - normed * jnp.mean(grad_out * normed, axis=-1, keepdims=True))
    grad_rows = grad_mixed.astype(jnp.bfloat16)
    widened = lax.optimization_barrier(grad_rows).astype(jnp.float32)
    row_dots = jnp.stack(
        [jnp.sum(widened * first, axis=-1), jnp.sum(widened * second, axis=-1)], axis=-1
    )
    return (grad_rows.reshape(count, head_count * DV), row_dots.reshape(count, head_count * 2))


def block_grads(
    query_rows, grad_rows, lse_rows, dot_rows, query_pos, key_rows, value_rows, key_pos, head_lambda
):
    count = query_rows.shape[0]
    width = key_rows.shape[0]
    head_count = head_lambda.shape[0]
    score_scale = DH ** (-0.5)
    query_heads = query_rows.reshape(count, head_count, 2, DH)
    key_heads = key_rows.reshape(width, head_count, 2, DH)
    grad_heads = grad_rows.reshape(count, head_count, DV)
    value_heads = value_rows.reshape(width, head_count, DV)
    scores = (
        jnp.einsum("nhad,mhad->hanm", query_heads, key_heads, preferred_element_type=jnp.float32)
        * score_scale
    )
    causal = query_pos[:, None] >= key_pos[None, :]
    shifts = lse_rows.reshape(count, head_count, 2).transpose(1, 2, 0)[..., None]
    probs = jnp.exp(jnp.where(causal, scores - shifts, -1e30))
    d_attn = jnp.einsum("nhe,mhe->hnm", grad_heads, value_heads, preferred_element_type=jnp.float32)
    dots = dot_rows.reshape(count, head_count, 2).transpose(1, 2, 0)[..., None]
    map_weight = jnp.stack([jnp.ones_like(head_lambda), -head_lambda], axis=1)[:, :, None, None]
    d_scores = (map_weight * probs * (d_attn[:, None] - dots)).astype(jnp.bfloat16)
    weights = (probs[:, 0] - head_lambda[:, None, None] * probs[:, 1]).astype(jnp.bfloat16)
    grad_q = (
        jnp.einsum("hanm,mhad->nhad", d_scores, key_heads, preferred_element_type=jnp.float32)
        * score_scale
    )
    grad_k = (
        jnp.einsum("hanm,nhad->mhad", d_scores, query_heads, preferred_element_type=jnp.float32)
        * score_scale
    )
    grad_v = jnp.einsum("hnm,nhe->mhe", weights, grad_heads, preferred_element_type=jnp.float32)
    return (grad_q.reshape(count, -1), grad_k.reshape(width, -1), grad_v.reshape(width, -1))


def per_device(
    queries,
    key_vectors,
    latents,
    value_weight,
    log_sums,
    out_first,
    out_second,
    cotangent,
    head_lambda,
):
    local_rows = queries.shape[0]
    offset = lax.axis_index("sp") * local_rows
    positions = offset + jnp.arange(local_rows, dtype=jnp.int32)
    last_row = offset + local_rows - 1
    values = jnp.dot(latents, value_weight, preferred_element_type=jnp.float32).astype(jnp.bfloat16)
    grad_rows, row_dots = row_terms(out_first, out_second, cotangent, head_lambda)
    gathered_stats = (
        lax.all_gather(log_sums, "sp", axis=0, tiled=True),
        lax.all_gather(row_dots, "sp", axis=0, tiled=True),
    )
    key_rows = lax.all_gather(key_vectors, "sp", axis=0, tiled=True)
    value_rows = lax.all_gather(values, "sp", axis=0, tiled=True)
    count = key_rows.shape[0]

    def compute(current):
        key_pos = jnp.arange(count, dtype=jnp.int32)
        grad_q, unused_k, unused_v = block_grads(
            queries,
            grad_rows,
            log_sums,
            row_dots,
            positions,
            key_rows,
            value_rows,
            key_pos,
            head_lambda,
        )
        return grad_q

    grad_queries = lax.cond(
        jnp.int32(0) <= last_row,
        compute,
        lambda current: current,
        jnp.zeros((local_rows, queries.shape[1]), jnp.float32),
    )
    start_totals = (
        jnp.zeros((local_rows, key_vectors.shape[1]), jnp.float32),
        jnp.zeros((local_rows, values.shape[1]), jnp.float32),
    )
    query_rows = lax.all_gather(queries, "sp", axis=0, tiled=True)
    grad_piece = lax.all_gather(grad_rows, "sp", axis=0, tiled=True)
    add_count = query_rows.shape[0]

    def compute(current):
        query_pos = jnp.arange(add_count, dtype=jnp.int32)
        lse_rows = gathered_stats[0]
        dot_rows = gathered_stats[1]
        unused_q, grad_k, grad_v = block_grads(
            query_rows,
            grad_piece,
            lse_rows,
            dot_rows,
            query_pos,
            key_vectors,
            values,
            positions,
            head_lambda,
        )
        return (grad_k, grad_v)

    grad_keys, grad_values = lax.cond(
        jnp.int32(0) + add_count - 1 >= offset, compute, lambda current: current, start_totals
    )
    values_grad = grad_values.astype(jnp.bfloat16)
    grad_weight = lax.psum_scatter(
        lax.dot_general(
            latents, values_grad, (((0,), (0,)), ((), ())), preferred_element_type=jnp.float32
        ).astype(jnp.bfloat16),
        "sp",
        scatter_dimension=0,
        tiled=True,
    ).astype(jnp.float32)
    latent_partial = lax.dot_general(
        values_grad, value_weight, (((1,), (1,)), ((), ())), preferred_element_type=jnp.float32
    )
    grad_latents = lax.psum_scatter(
        latent_partial.astype(jnp.bfloat16), "tp", scatter_dimension=1, tiled=True
    )
    return (grad_queries, grad_keys, grad_latents, grad_weight)


def solution(mesh):
    return jax.shard_map(
        per_device,
        mesh=mesh,
        in_specs=(
            P("sp", "tp"),
            P("sp", "tp"),
            P("sp", None),
            P(None, "tp"),
            P("sp", "tp"),
            P("sp", "tp"),
            P("sp", "tp"),
            P("sp", "tp"),
            P("tp"),
        ),
        out_specs=(P("sp", "tp"), P("sp", "tp"), P("sp", "tp"), P("sp", "tp")),
        check_vma=False,
    )
```

profile of v0, /device:TPU:0, one launch (start us, length us, event | category | flops | bytes accessed | tf_op | source)
XLA Modules:
  0.0 336.8 jit_solution(91147204040858790)
XLA Ops:
  7.2 0.9 broadcast_bitcast_fusion
  8.1 1.2 convert_bitcast_fusion.1
  9.3 1.6 multiply_reduce_fusion
  10.9 0.1 copy.163
  11.1 1.6 fusion.38
  12.7 0.8 copy.164
  13.5 1.3 mul.122.clone
  14.8 0.4 mul.119.clone
  15.2 2.1 fusion.33
  17.4 0.7 all-gather.11.cloned.1.call-update
  18.1 2.8 convolution_convert_fusion.2
  21.0 0.5 all-gather.7.cloned.1.call-update
  21.6 1.5 fusion.37
  23.1 0.5 fusion.34
  23.6 0.2 copy-done.1
  23.8 0.1 copy.161
  23.9 0.2 copy.162
  24.1 0.1 copy.147
  24.3 33.1 %all-gather.1 = f32[8,288,8]{1,2,0:T(8,128)S(1)} all-gather(f32[1,288,8]{1,2,0:T(8,128)S(1)} %reshape.93), channel_id=1, replica_groups=mesh['sp'=8,'tp'=4] {'sp'}, dimensions={0}, use_global_device_ids=true | all-gather | bytes 82944 | tf_op jit(solution)/shard_map/all_gather | solution.py:82
  57.5 31.1 %all-gather = f32[8,288,8]{1,2,0:T(8,128)S(1)} all-gather(f32[1,288,8]{1,2,0:T(8,128)S(1)} %bitcast.156), channel_id=1, replica_groups=mesh['sp'=8,'tp'=4] {'sp'}, dimensions={0}, use_global_device_ids=true | all-gather | bytes 82944 | tf_op jit(solution)/shard_map/all_gather | solution.py:81
  88.7 37.1 %all-gather.11.cloned.1.call-done = bf16[2304,512]{1,0:T(8,128)(2,1)} async-done(((bf16[288,512]{1,0:T(8,128)(2,1)}), bf16[2304,512]{1,0:T(8,128)(2,1)}) %all-gather.11.cloned.1.call-update) | async-done | bytes 2359312 | tf_op jit(solution)/shard_map/all_gather | solution.py:113
  125.8 47.3 %conditional.3 = (bf16[288,512]{1,0:T(8,128)(2,1)}, f32[288,512]{1,0:T(8,128)}) conditional(s32[]{:T(128)} %convert_element_type.67, () %tuple.26, (f32[4]{0:T(128)S(1)}, s32[288]{0:T(512)S(1)}, bf16[2304,512]{1,0:T(8,128)(2,1)}, bf16[288,512]{1,0:T(8,128)(2,1)}, f32[2304,8]{0,1:T(8,128)S(1)}, /*index=5*/bf16[2304,512]{1,0:T(8,128)(2,1)}, ...), branch_computations={%region_6.7_spmd, %region_7.8_spmd} | conditional | flops 2763988992 | bytes 116491648 | solution.py:134
  125.8 4.4 %copy.149 = bf16[2304,512]{0,1:T(8,128)(2,1)} copy(bf16[2304,512]{1,0:T(8,128)(2,1)} %get-tuple-element.162) | data formatting | bytes 4718592 | tf_op jit(solution)/shard_map
  130.2 1.3 iota_compare_fusion.1
  131.5 0.2 copy.150
  131.8 11.4 %select_exponential_fusion = f32[4,2,2304,288]{2,3,1,0:T(8,128)} fusion(bf16[2304,4,2,64]{0,3,2,1:T(8,128)(2,1)} %bitcast.143, bf16[288,4,2,64]{0,3,2,1:T(8,128)(2,1)S(1)} %bitcast.153, f32[4,2,2304]{2,1,0:T(2,128)S(1)} %bitcast.155, pred[2304,288]{0,1:T(8,128)(4,1)} %iota_compare_fusion.1), kind=kOutput, calls=%fused_computation.10 | convolution fusion | flops 695402496 | bytes 24625152 | tf_op jit(solution)/shard_map/cond/branch_1_fun/nhad,mhad->hanm/dot_general | solution.py:40
  143.2 5.5 %fusion.12 = f32[4,2304,288]{1,2,0:T(8,128)} fusion(bf16[2304,512]{1,0:T(8,128)(2,1)S(1)} %copy-done.3, bf16[288,512]{1,0:T(8,128)(2,1)S(1)} %copy-done.4), kind=kOutput, calls=%fused_computation.20 | convolution fusion | flops 679477248 | bytes 13271040 | tf_op jit(solution)/shard_map/cond/branch_1_fun/nhe,mhe->hnm/dot_general | solution.py:46
  148.7 0.1 copy.160
  149.0 13.0 %fusion.16 = f32[4,2,288,64]{2,3,1,0:T(8,128)S(1)} fusion(bf16[2304,4,2,64]{0,3,2,1:T(8,128)(2,1)} %bitcast.144, f32[4,2,2304,288]{2,3,1,0:T(8,128)} %select_exponential_fusion, f32[4,2,2304]{2,1,0:T(2,128)S(1)} %bitcast.154, f32[4,2304,288]{1,2,0:T(8,128)} %fusion.12, f32[4,2]{1,0:T(4,128)S(1)} %stack.17.clone), kind=kOutput, calls=%fused_computation.24 | convolution fusion | flops 700858368 | bytes 34873376 | tf_op jit(solution)/shard_map/cond/branch_1_fun/hanm,nhad->mhad/dot_general | solution.py:56
  162.0 1.1 copy.157
  163.0 9.4 %fusion.22 = bf16[4,36,8,128]{3,2,1,0:T(8,128)(2,1)S(1)} fusion(f32[4,2,2304,288]{2,3,1,0:T(8,128)} %select_exponential_fusion, f32[4]{0:T(128)S(1)} %get-tuple-element.44, bf16[2304,512]{1,0:T(8,128)(2,1)} %get-tuple-element.49), kind=kOutput, calls=%fused_computation.26 | convolution fusion | flops 687587328 | bytes 23887888 | tf_op jit(solution)/shard_map/cond/branch_1_fun/hnm,nhe->mhe/dot_general | solution.py:59
  172.4 0.8 copy.205
  173.2 4.0 %fusion.29 = bf16[2048,512]{0,1:T(8,128)(2,1)} fusion(bf16[288,512]{1,0:T(8,128)(2,1)} %get-tuple-element.59, bf16[288,2048]{1,0:T(8,128)(2,1)} %param.15), kind=kOutput, calls=%fused_computation.32 | convolution fusion | flops 605028352 | bytes 3571712 | tf_op jit(solution)/shard_map/dot_general | solution.py:139
  177.2 0.3 reduce-scatter.3.cloned.1.call-start
  177.5 2.8 convolution_convert_fusion.1
  180.4 51.1 %all-gather.7.cloned.1.call-done = bf16[2304,512]{1,0:T(8,128)(2,1)} async-done(((bf16[288,512]{1,0:T(8,128)(2,1)}), bf16[2304,512]{1,0:T(8,128)(2,1)}) %all-gather.7.cloned.1.call-update) | async-done | bytes 2359312 | tf_op jit(solution)/shard_map/all_gather | solution.py:84
  231.4 29.7 %conditional.2 = (f32[288,512]{1,0:T(8,128)}) conditional(s32[]{:T(128)} %convert_element_type.60, () %tuple.24, (f32[4]{0:T(128)S(1)}, s32[288]{0:T(512)S(1)}, bf16[288,512]{1,0:T(8,128)(2,1)S(1)}, bf16[2304,512]{1,0:T(8,128)(2,1)}, f32[288,8]{0,1:T(8,128)S(1)}, /*index=5*/bf16[2304,512]{1,0:T(8,128)(2,1)}, bf16[288,4,128]{2,0,1:T(8,128)(2,1)S(1)}, ...), branch_computations={%region_4.0_spmd, %region_5.6_spmd} | conditional | flops 2076401664 | bytes 35003676 | solution.py:103
  231.4 7.3 %fusion = f32[4,288,2304]{2,1,0:T(8,128)} fusion(bf16[288,4,128]{2,0,1:T(8,128)(2,1)S(1)} %get-tuple-element.41, bf16[2304,512]{1,0:T(8,128)(2,1)} %get-tuple-element.42), kind=kOutput, calls=%fused_computation.2 | convolution fusion | flops 679477248 | bytes 13271040 | tf_op jit(solution)/shard_map/cond/branch_1_fun/nhe,mhe->hnm/dot_general | solution.py:46
  238.7 4.3 %copy.142 = bf16[2304,512]{0,1:T(8,128)(2,1)} copy(bf16[2304,512]{1,0:T(8,128)(2,1)} %get-tuple-element.155) | data formatting | bytes 4718592 | tf_op jit(solution)/shard_map
  243.0 1.3 iota_compare_fusion
  244.3 0.9 copy.141
  245.2 0.1 copy.143
  245.4 0.1 copy.158
  245.6 14.5 %convolution_multiply_fusion = f32[4,2,288,64]{2,3,1,0:T(8,128)S(1)} fusion(bf16[2304,4,2,64]{0,3,2,1:T(8,128)(2,1)} %bitcast.146, bf16[288,4,2,64]{0,3,2,1:T(8,128)(2,1)} %bitcast.152, f32[4,2,288]{2,1,0:T(2,128)S(1)} %bitcast.157, f32[4,288,2304]{2,1,0:T(8,128)} %fusion, f32[4,2,288]{2,1,0:T(2,128)S(1)} %bitcast.158, f32[4,2]{1,0:T(4,128)S(1)} %stack.15.clone, ...), kind=kOutput, calls=%fused_computation.5 | convolution fusion | flops 1396260864 | bytes 14542880 | tf_op jit(solution)/shard_map/cond/branch_1_fun/hanm,mhad->nhad/dot_general | solution.py:52
  260.0 1.1 copy.155
  261.1 41.2 %reduce-scatter.5.cloned.1.call-done = bf16[256,512]{0,1:T(8,128)(2,1)} async-done(((bf16[2048,512]{0,1:T(8,128)(2,1)}), bf16[256,512]{0,1:T(8,128)(2,1)}) %reduce-scatter.5.cloned.1.call-update) | async-done | bytes 262160 | tf_op jit(solution)/shard_map/reduce_scatter | solution.py:138
  302.3 1.9 copy.153
  304.2 25.8 %reduce-scatter.3.cloned.1.call-done = bf16[288,512]{1,0:T(8,128)(2,1)} async-done(((bf16[288,2048]{1,0:T(8,128)(2,1)}), bf16[288,512]{1,0:T(8,128)(2,1)}) %reduce-scatter.3.cloned.1.call-update) | async-done | bytes 294928 | tf_op jit(solution)/shard_map/reduce_scatter | solution.py:149
  (46 shorter events, 0.9 us)
Async XLA Ops:
  7.2 11.0 %copy-start = (bf16[2048,512]{1,0:T(8,128)(2,1)S(1)}, bf16[2048,512]{1,0:T(8,128)(2,1)}, u32[]{:S(2)}) copy-start(bf16[2048,512]{1,0:T(8,128)(2,1)} %param.16) | copy-start | bytes 6291460
  7.2 81.5 %all-gather.13.cloned.1.call-start = ((), (), s32[]{:S(2)}) async-start(), calls=%async_computation.5 | async-start | bytes 2654208 | tf_op jit(solution)/shard_map/all_gather | solution.py:114
  17.3 108.5 %all-gather.11.cloned.1.call-start = ((), (), s32[]{:S(2)}) async-start(), calls=%async_computation.4 | async-start | bytes 2654208 | tf_op jit(solution)/shard_map/all_gather | solution.py:113
  18.1 162.3 %all-gather.9.cloned.1.call-start = ((), (), s32[]{:S(2)}) async-start(), calls=%async_computation.3 | async-start | bytes 2654208 | tf_op jit(solution)/shard_map/all_gather | solution.py:85
  20.9 36.6 %copy-start.7 = (f32[288,8]{0,1:T(8,128)S(1)}, f32[288,8]{0,1:T(8,128)}, u32[]{:S(2)}) copy-start(f32[288,8]{0,1:T(8,128)} %param.17) | copy-start | bytes 27652
  20.9 104.9 %copy-start.9 = (f32[4]{0:T(128)S(1)}, f32[4]{0:T(128)}, u32[]{:S(2)}) copy-start(f32[4]{0:T(128)} %param.21) | copy-start | bytes 52
  20.9 210.5 %all-gather.7.cloned.1.call-start = ((), (), s32[]{:S(2)}) async-start(), calls=%async_computation.2 | async-start | bytes 2654208 | tf_op jit(solution)/shard_map/all_gather | solution.py:84
  21.5 280.8 %reduce-scatter.5.cloned.1.call-start = ((), (), s32[]{:S(2)}) async-start(), calls=%async_computation.7 | async-start | bytes 2359296 | tf_op jit(solution)/shard_map/reduce_scatter | solution.py:138
  23.1 0.7 copy-start.1
  125.8 5.6 %copy-start.5 = (bf16[288,512]{1,0:T(8,128)(2,1)S(1)}, bf16[288,512]{1,0:T(8,128)(2,1)}, u32[]{:S(2)}) copy-start(bf16[288,512]{1,0:T(8,128)(2,1)} %get-tuple-element.163) | copy-start | bytes 884740 | tf_op jit(solution)/shard_map/cond
  131.8 11.4 %copy-start.3 = (bf16[2304,512]{1,0:T(8,128)(2,1)S(1)}, bf16[2304,512]{1,0:T(8,128)(2,1)}, u32[]{:S(2)}) copy-start(bf16[2304,512]{1,0:T(8,128)(2,1)} %get-tuple-element.49) | copy-start | bytes 7077892 | tf_op jit(solution)/shard_map/cond
  131.8 11.4 %copy-start.4 = (bf16[288,512]{1,0:T(8,128)(2,1)S(1)}, bf16[288,512]{1,0:T(8,128)(2,1)}, u32[]{:S(2)}) copy-start(bf16[288,512]{1,0:T(8,128)(2,1)} %get-tuple-element.50) | copy-start | bytes 884740 | tf_op jit(solution)/shard_map/cond
  177.2 54.2 %copy-start.2 = (bf16[288,4,128]{2,0,1:T(8,128)(2,1)S(1)}, bf16[288,4,128]{2,0,1:T(8,128)(2,1)}, u32[]{:S(2)}) copy-start(bf16[288,4,128]{2,0,1:T(8,128)(2,1)} %copy-done.1) | copy-start | bytes 884740
  177.2 54.2 %copy-start.6 = (bf16[288,512]{1,0:T(8,128)(2,1)S(1)}, bf16[288,512]{1,0:T(8,128)(2,1)}, u32[]{:S(2)}) copy-start(bf16[288,512]{1,0:T(8,128)(2,1)} %param.13) | copy-start | bytes 884740
  177.2 54.2 %copy-start.8 = (f32[288,8]{0,1:T(8,128)S(1)}, f32[288,8]{0,1:T(8,128)}, u32[]{:S(2)}) copy-start(f32[288,8]{0,1:T(8,128)} %param.17) | copy-start | bytes 27652
  177.2 152.7 %reduce-scatter.3.cloned.1.call-start = ((), (), s32[]{:S(2)}) async-start(), calls=%async_computation.6 | async-start | bytes 1474560 | tf_op jit(solution)/shard_map/reduce_scatter | solution.py:149
Sparse Core Ops, SparseCore 0:
  17.4 55.7 all-gather.12
  75.4 50.4 all-gather.10
  128.6 50.3 all-gather.8
  181.0 50.3 all-gather.6
  234.8 67.4 reduce-scatter.4
  305.3 24.6 reduce-scatter.2
where the time goes:
time: 337 us
  waiting for transfers between devices  156 us (46%)
  matrix products  70.6 us (21%)
  blocking collectives  64.1 us (19%)
  local copies, waits for them, and re-layouts  19.6 us (6%)
  between operations  14.3 us (4%)
  other arithmetic  11.2 us (3%)
    all_gather x1, waiting for transfers between devices, per_device(): key_rows = lax.all_gather(key_vectors, 'sp', axis=0, tiled=True)  51.1 us
    reduce_scatter x1, waiting for transfers between devices, per_device(): lax.psum_scatter(lax.dot_general(latents, values_grad, (((0,), (0,)), (()...  41.2 us
    all_gather x1, waiting for transfers between devices, per_device(): query_rows = lax.all_gather(queries, 'sp', axis=0, tiled=True)  37.1 us
    all_gather x1, blocking collectives, per_device(): lax.all_gather(row_dots, 'sp', axis=0, tiled=True)  33.1 us
    all_gather x1, blocking collectives, per_device(): lax.all_gather(log_sums, 'sp', axis=0, tiled=True)  31.1 us
    reduce_scatter x1, waiting for transfers between devices, per_device(): lax.psum_scatter(latent_partial.astype(jnp.bfloat16), 'tp', scatter_dimen...  25.8 us
    dot_general x1, matrix products, block_grads(): jnp.einsum('hanm,mhad->nhad', d_scores, key_heads, preferred_element_type...  14.5 us
    dot_general x1, matrix products, block_grads(): jnp.einsum('hanm,nhad->mhad', d_scores, query_heads, preferred_element_ty...  13 us
  transfers between devices with their start and end apart: 6, of which 4 were waited for; matrix products, arithmetic and copies ran while one was open for 27% of the time, Pallas kernels for 0%

commit v1 on v0

--- a/solution.py
+++ b/solution.py
@@ -1,10 +1,15 @@
+import functools
+
 import jax
 import jax.numpy as jnp
 from jax import lax
+from jax.experimental import pallas as pl
+from jax.experimental.pallas import tpu as pltpu
 from jax.sharding import PartitionSpec as P
 
 DH = 64
 DV = 128
+BLOCK = 256
 
 
 def row_terms(out_first, out_second, cotangent, head_lambda):
@@ -152,9 +157,384 @@
     return (grad_queries, grad_keys, grad_latents, grad_weight)
 
 
+def exchange_kernel(axis, n, parts, *refs):
+    swap_blocks(axis, n, refs[:parts], refs[parts : 2 * parts], *refs[2 * parts :])
+
+
+def swap_blocks(axis, n, ins, outs, send_sem, recv_sem, local_sem, prepare=lambda: None):
+    parts = len(ins)
+    me = lax.axis_index(axis)
+    barrier = pltpu.get_barrier_semaphore()
+    for step in range(1, n):
+        peer = lax.rem(me + step, n)
+        pl.semaphore_signal(
+            barrier, inc=1, device_id={axis: peer}, device_id_type=pl.DeviceIdType.MESH
+        )
+    prepare()
+    pl.semaphore_wait(barrier, n - 1)
+
+    def remote(part, step, slot):
+        peer = lax.rem(me + step, n)
+        return pltpu.make_async_remote_copy(
+            src_ref=ins[part].at[peer],
+            dst_ref=outs[part].at[slot],
+            send_sem=send_sem.at[part, step],
+            recv_sem=recv_sem.at[part, step],
+            device_id={axis: peer},
+            device_id_type=pl.DeviceIdType.MESH,
+        )
+
+    order = sorted(range(1, n), key=lambda step: -min(step, n - step))
+    for part in reversed(range(parts)):
+        for step in order:
+            remote(part, step, me).start()
+    for part in range(parts):
+        own = pltpu.make_async_copy(ins[part].at[me], outs[part].at[me], local_sem.at[part])
+        own.start()
+        own.wait()
+    for part in range(parts):
+        for step in order:
+            remote(part, step, lax.rem(me + n - step, n)).wait_recv()
+    for part in range(parts):
+        for step in order:
+            remote(part, step, me).wait_send()
+
+
+def exchange(arrays, axis, n, collective_id):
+    parts = len(arrays)
+    sent = sum(a.size * a.dtype.itemsize for a in arrays)
+    return pl.pallas_call(
+        functools.partial(exchange_kernel, axis, n, parts),
+        out_shape=[jax.ShapeDtypeStruct(a.shape, a.dtype) for a in arrays],
+        in_specs=[pl.BlockSpec(memory_space=pltpu.VMEM)] * parts,
+        out_specs=[pl.BlockSpec(memory_space=pltpu.VMEM)] * parts,
+        scratch_shapes=[
+            pltpu.SemaphoreType.DMA((parts, n)),
+            pltpu.SemaphoreType.DMA((parts, n)),
+            pltpu.SemaphoreType.DMA((parts,)),
+        ],
+        compiler_params=pltpu.CompilerParams(collective_id=collective_id, has_side_effects=True),
+        cost_estimate=pl.CostEstimate(flops=0, bytes_accessed=sent * 16, transcendentals=0),
+    )(*arrays)
+
+
+def head_of(index):
+    return slice(index * DV, (index + 1) * DV)
+
+
+def send_kernel(
+    axis, n, q_ref, k_ref, v_ref, first_ref, second_ref, cot_ref, lse_ref, lambda_ref,
+    x_out, stats_out, x_s, stats_s, *sems
+):
+    def prepare():
+        score_scale = jnp.bfloat16(DH**-0.5)
+        columns = []
+        stats_s[...] = jnp.zeros_like(stats_s)
+        for head in range(n // 2):
+            lanes = head_of(head)
+            first = first_ref[:, lanes].astype(jnp.float32)
+            second = second_ref[:, lanes].astype(jnp.float32)
+            mixed = first - lambda_ref[head] * second
+            inverse = lax.rsqrt(jnp.mean(mixed * mixed, axis=-1, keepdims=True) + 1e-06)
+            normed = mixed * inverse
+            grad_out = cot_ref[:, lanes].astype(jnp.float32)
+            mean_dot = jnp.mean(grad_out * normed, axis=-1, keepdims=True)
+            grad_rows = (inverse * (grad_out - normed * mean_dot)).astype(jnp.bfloat16)
+            widened = grad_rows.astype(jnp.float32)
+            columns.append(jnp.sum(widened * first, axis=-1, keepdims=True))
+            columns.append(jnp.sum(widened * second, axis=-1, keepdims=True))
+            q_pair = q_ref[:, lanes] * score_scale
+            k_pair = k_ref[:, lanes]
+            for m in range(2):
+                unit = 2 * head + m
+                half = slice(m * DH, (m + 1) * DH)
+                x_s[unit, :, 0 : 2 * DH] = jnp.concatenate(
+                    [q_pair[:, half], k_pair[:, half]], axis=1
+                )
+                x_s[unit, :, 2 * DH : 2 * DH + DV] = v_ref[:, lanes]
+                x_s[unit, :, 2 * DH + DV :] = grad_rows
+        dots = jnp.concatenate(columns, axis=1).T
+        for unit in range(n):
+            stats_s[unit, 0:1, :] = lse_ref[unit : unit + 1, :]
+            stats_s[unit, 1:2, :] = dots[unit : unit + 1, :]
+
+    swap_blocks(axis, n, (x_s, stats_s), (x_out, stats_out), *sems, prepare=prepare)
+
+
+def send_units(queries, keys, values, first, second, cotangent, lse, head_lambda, n):
+    rows = queries.shape[0]
+    shapes = [((n, rows, 2 * DH + 2 * DV), jnp.bfloat16), ((n, 8, rows), jnp.float32)]
+    vmem = pl.BlockSpec(memory_space=pltpu.VMEM)
+    return pl.pallas_call(
+        functools.partial(send_kernel, "sp", n),
+        out_shape=[jax.ShapeDtypeStruct(*shape) for shape in shapes],
+        in_specs=[vmem] * 7 + [pl.BlockSpec(memory_space=pltpu.SMEM)],
+        out_specs=[vmem] * 2,
+        scratch_shapes=[pltpu.VMEM(*shape) for shape in shapes]
+        + [
+            pltpu.SemaphoreType.DMA((2, n)),
+            pltpu.SemaphoreType.DMA((2, n)),
+            pltpu.SemaphoreType.DMA((2,)),
+        ],
+        compiler_params=pltpu.CompilerParams(collective_id=1, has_side_effects=True),
+        cost_estimate=pl.CostEstimate(
+            flops=0, bytes_accessed=queries.size * 64, transcendentals=0
+        ),
+    )(queries, keys, values, first, second, cotangent, lse, head_lambda)
+
+
+def unpack_kernel(x_ref, lambda_ref, q_ref, k_ref, v_ref):
+    for head in range(x_ref.shape[0] // 2):
+        lanes = head_of(head)
+        weight = -lambda_ref[head]
+        first = x_ref[2 * head].astype(jnp.float32)
+        second = x_ref[2 * head + 1].astype(jnp.float32) * weight
+        q_ref[:, lanes] = jnp.concatenate([first[:, :DH], second[:, :DH]], axis=1) * DH ** (-0.5)
+        k_ref[:, lanes] = jnp.concatenate(
+            [first[:, DH : 2 * DH], second[:, DH : 2 * DH]], axis=1
+        )
+        v_ref[:, lanes] = (first[:, 2 * DH :] + second[:, 2 * DH :]).astype(jnp.bfloat16)
+
+
+def unpack(grads, head_lambda):
+    n, rows, _ = grads.shape
+    vmem = pl.BlockSpec(memory_space=pltpu.VMEM)
+    kinds = (jnp.float32, jnp.float32, jnp.bfloat16)
+    return pl.pallas_call(
+        unpack_kernel,
+        out_shape=[jax.ShapeDtypeStruct((rows, n * DH), kind) for kind in kinds],
+        in_specs=[vmem, pl.BlockSpec(memory_space=pltpu.SMEM)],
+        out_specs=[vmem] * 3,
+        cost_estimate=pl.CostEstimate(flops=0, bytes_accessed=grads.size * 6, transcendentals=0),
+    )(grads, head_lambda)
+
+
+def attention_kernel(block, x_ref, stats_ref, o_ref, q_s, k_s, kt_s, dqt_s, dk_s, dv_s):
+    blocks = x_ref.shape[0] // block
+
+    def rows_of(index):
+        return pl.ds(pl.multiple_of(index * block, block), block)
+
+    def prologue(index, carry):
+        rows = rows_of(index)
+        pair = x_ref[rows, 0 : 2 * DH]
+        q_s[rows, :] = pair[:, :DH]
+        keys = pair[:, DH:]
+        k_s[rows, :] = keys
+        kt_s[index] = keys.T
+        dqt_s[index] = jnp.zeros((DH, block), jnp.float32)
+        return carry
+
+    lax.fori_loop(0, blocks, prologue, 0)
+
+    def tile(key_index, query_index, diagonal):
+        key_rows, query_rows = rows_of(key_index), rows_of(query_index)
+        queries = q_s[query_rows, :]
+        grads = x_ref[query_rows, 2 * DH + DV :]
+        nt = (((1,), (1,)), ((), ()))
+        scores = lax.dot_general(
+            k_s[key_rows, :], queries, nt, preferred_element_type=jnp.float32
+        )
+        stats = stats_ref[query_index]
+        shifted = scores - stats[0:1, :]
+        if diagonal:
+            key_at = lax.broadcasted_iota(jnp.int32, (block, block), 0)
+            query_at = lax.broadcasted_iota(jnp.int32, (block, block), 1)
+            shifted = jnp.where(query_at >= key_at, shifted, -1e30)
+        probs = jnp.exp(shifted)
+        d_attn = lax.dot_general(
+            x_ref[key_rows, 2 * DH : 2 * DH + DV], grads, nt, preferred_element_type=jnp.float32
+        )
+        d_scores = (probs * (d_attn - stats[1:2, :])).astype(jnp.bfloat16)
+        weights = probs.astype(jnp.bfloat16)
+        dk = jnp.dot(d_scores, queries, preferred_element_type=jnp.float32)
+        dv = jnp.dot(weights, grads, preferred_element_type=jnp.float32)
+        dqt_s[query_index] += jnp.dot(
+            kt_s[key_index], d_scores, preferred_element_type=jnp.float32
+        )
+        if diagonal:
+            dk_s[...] = dk
+            dv_s[...] = dv
+        else:
+            dk_s[...] += dk
+            dv_s[...] += dv
+
+    def column(key_index, carry):
+        tile(key_index, key_index, True)
+
+        def inner(query_index, carry):
+            tile(key_index, query_index, False)
+            return carry
+
+        lax.fori_loop(key_index + 1, blocks, inner, 0)
+        out = [dqt_s[key_index].T, dk_s[...], dv_s[...]]
+        o_ref[rows_of(key_index), :] = jnp.concatenate(out, axis=1).astype(jnp.bfloat16)
+        return carry
+
+    lax.fori_loop(0, blocks, column, 0)
+
+
+def attention(x, stats, block):
+    count = x.shape[0]
+    pairs = count * (count + block) // 2
+    return pl.pallas_call(
+        functools.partial(attention_kernel, block),
+        out_shape=jax.ShapeDtypeStruct((count, 2 * DH + DV), jnp.bfloat16),
+        in_specs=[pl.BlockSpec(memory_space=pltpu.VMEM)] * 2,
+        out_specs=pl.BlockSpec(memory_space=pltpu.VMEM),
+        scratch_shapes=[
+            pltpu.VMEM((count, DH), jnp.bfloat16),
+            pltpu.VMEM((count, DH), jnp.bfloat16),
+            pltpu.VMEM((count // block, DH, block), jnp.bfloat16),
+            pltpu.VMEM((count // block, DH, block), jnp.float32),
+            pltpu.VMEM((block, DH), jnp.float32),
+            pltpu.VMEM((block, DV), jnp.float32),
+        ],
+        cost_estimate=pl.CostEstimate(
+            flops=2 * pairs * 448, bytes_accessed=count * 1600, transcendentals=pairs
+        ),
+    )(x, stats)
+
+
+def weight_kernel(
+    axis, n, lat_ref, dv_ref, o_ref, to_pair, from_pair, sums, from_line,
+    pair_send, pair_recv, line_send, line_recv
+):
+    line = n // 2
+    me = lax.axis_index(axis)
+    place, side = me // 2, lax.rem(me, 2)
+    partner = 2 * place + 1 - side
+    width = lat_ref.shape[1] // n
+    mesh_id = pl.DeviceIdType.MESH
+
+    def at(step):
+        return lax.rem(place + step, line)
+
+    def term(unit):
+        columns = pl.ds(pl.multiple_of(unit * width, width), width)
+        return lax.dot_general(
+            lat_ref[:, columns],
+            dv_ref[...],
+            (((0,), (0,)), ((), ())),
+            preferred_element_type=jnp.float32,
+        )
+
+    def pair_copy(step):
+        return pltpu.make_async_remote_copy(
+            src_ref=to_pair.at[step],
+            dst_ref=from_pair.at[step],
+            send_sem=pair_send.at[step],
+            recv_sem=pair_recv.at[step],
+            device_id={axis: partner},
+            device_id_type=mesh_id,
+        )
+
+    def line_copy(step):
+        return pltpu.make_async_remote_copy(
+            src_ref=sums.at[step],
+            dst_ref=from_line.at[step],
+            send_sem=line_send.at[step],
+            recv_sem=line_recv.at[step],
+            device_id={axis: 2 * at(step) + side},
+            device_id_type=mesh_id,
+        )
+
+    barrier = pltpu.get_barrier_semaphore()
+    pl.semaphore_signal(barrier, inc=1, device_id={axis: partner}, device_id_type=mesh_id)
+    for step in range(1, line):
+        pl.semaphore_signal(
+            barrier, inc=1, device_id={axis: 2 * at(step) + side}, device_id_type=mesh_id
+        )
+    order = sorted(range(1, line), key=lambda step: -min(step, line - step)) + [0]
+    to_pair[order[0]] = term(2 * at(order[0]) + 1 - side).astype(jnp.bfloat16)
+    pl.semaphore_wait(barrier, line)
+    pair_copy(order[0]).start()
+    for step in order[1:]:
+        to_pair[step] = term(2 * at(step) + 1 - side).astype(jnp.bfloat16)
+        pair_copy(step).start()
+    for step in order:
+        own = term(2 * at(step) + side)
+        pair_copy(step).wait_recv()
+        total = own + from_pair[step].astype(jnp.float32)
+        if step == 0:
+            o_ref[...] = total
+        else:
+            sums[step] = total.astype(jnp.bfloat16)
+            line_copy(step).start()
+    for step in order[:-1]:
+        line_copy(step).wait_recv()
+        o_ref[...] += from_line[step].astype(jnp.float32)
+    for step in order:
+        pair_copy(step).wait_send()
+    for step in order[:-1]:
+        line_copy(step).wait_send()
+
+
+def summed_weight(latents, values_grad, n):
+    rows, depth = latents.shape
+    columns = values_grad.shape[1]
+    width = depth // n
+    vmem = pl.BlockSpec(memory_space=pltpu.VMEM)
+    buffer = pltpu.VMEM((n // 2, width, columns), jnp.bfloat16)
+    return pl.pallas_call(
+        functools.partial(weight_kernel, "sp", n),
+        out_shape=jax.ShapeDtypeStruct((width, columns), jnp.float32),
+        in_specs=[vmem] * 2,
+        out_specs=vmem,
+        scratch_shapes=[buffer] * 4 + [pltpu.SemaphoreType.DMA((n // 2,))] * 4,
+        compiler_params=pltpu.CompilerParams(collective_id=3, has_side_effects=True),
+        cost_estimate=pl.CostEstimate(
+            flops=2 * rows * depth * columns,
+            bytes_accessed=depth * columns * 64,
+            transcendentals=0,
+        ),
+    )(latents, values_grad)
+
+
+def by_unit(
+    queries,
+    key_vectors,
+    latents,
+    value_weight,
+    log_sums,
+    out_first,
+    out_second,
+    cotangent,
+    head_lambda,
+):
+    n = lax.axis_size("sp")
+    rows = queries.shape[0]
+    values = jnp.dot(latents, value_weight, preferred_element_type=jnp.float32).astype(jnp.bfloat16)
+    packed, stats = send_units(
+        queries, key_vectors, values, out_first, out_second, cotangent, log_sums.T, head_lambda, n
+    )
+    count = n * rows
+    stats = stats.transpose(1, 0, 2).reshape(8, count // BLOCK, BLOCK).transpose(1, 0, 2)
+    grads = attention(packed.reshape(count, 2 * DH + 2 * DV), stats, BLOCK)
+    (grads,) = exchange([grads.reshape(n, rows, 2 * DH + DV)], "sp", n, 2)
+    grad_queries, grad_keys, values_grad = unpack(grads, head_lambda)
+    latent_partial = lax.dot_general(
+        values_grad, value_weight, (((1,), (1,)), ((), ())), preferred_element_type=jnp.float32
+    )
+    grad_latents = lax.psum_scatter(
+        latent_partial.astype(jnp.bfloat16), "tp", scatter_dimension=1, tiled=True
+    )
+    grad_weight = summed_weight(latents, values_grad, n)
+    return (grad_queries, grad_keys, grad_latents, grad_weight)
+
+
+def dispatch(queries, key_vectors, latents, value_weight, log_sums, *rest):
+    n = lax.axis_size("sp")
+    count = n * queries.shape[0]
+    fits = rest[-1].shape[0] * 2 == n and count % BLOCK == 0
+    fits = fits and latents.shape[1] % (n * DV) == 0
+    run = by_unit if fits else per_device
+    return run(queries, key_vectors, latents, value_weight, log_sums, *rest)
+
+
 def solution(mesh):
     return jax.shard_map(
-        per_device,
+        dispatch,
         mesh=mesh,
         in_specs=(
             P("sp", "tp"),

time: 337 us -> 164 us (0.49)
  waiting for transfers between devices: 156 us -> 0.04 us
  Pallas kernels: 0 us -> 139 us
  matrix products: 70.6 us -> 5.54 us
  blocking collectives: 64.1 us -> 0 us
  local copies, waits for them, and re-layouts: 19.6 us -> 5.11 us
  other arithmetic: 11.2 us -> 0 us
    pallas_call x0 -> x5, Pallas kernels: none -> 139 us  [the longest x1 42 us: send_units(): pl.pallas_call(functools.partial(send_kernel, 'sp', n), out_shape=[jax.Sh...]
    all_gather x4 -> x0, waiting for transfers between devices: 88.2 us -> none  [the longest x1 51.1 us: per_device(): key_rows = lax.all_gather(key_vectors, 'sp', axis=0, tiled=True)]
    reduce_scatter x2 -> x1, waiting for transfers between devices: 67 us -> 0.02 us  [by_unit(): lax.psum_scatter(latent_partial.astype(jnp.bfloat16), 'tp', scatter_dimen...]
    dot_general x9 -> x2, matrix products: 70.6 us -> 5.54 us  [the longest x1 2.79 us: by_unit(): lax.dot_general(values_grad, value_weight, (((1,), (1,)), ((), ())), pref...]
    all_gather x2 -> x0, blocking collectives: 64.1 us -> none  [the longest x1 33.1 us: per_device(): lax.all_gather(row_dots, 'sp', axis=0, tiled=True)]
    another operation x8 -> x0, local copies, waits for them, and re-layouts: 10.3 us -> none
    reduce_sum x3 -> x0, other arithmetic: 3.76 us -> none  [the longest x1 1.65 us: row_terms(): inverse = lax.rsqrt(jnp.mean(mixed * mixed, axis=-1, keepdims=True) + 1e-06)]
    convert_element_type x2 -> x0, other arithmetic: 3.63 us -> none  [row_terms(): grad_rows = grad_mixed.astype(jnp.bfloat16)]
  transfers between devices with their start and end apart: 6 -> 1, of which waited for: 4 -> 0; matrix products, arithmetic and copies ran while one was open for 27% -> 0% of each run, Pallas kernels for 0% -> 23%
where the time goes in v1:
time: 164 us
  Pallas kernels  139 us (85%)
  between operations  14.1 us (9%)
  matrix products  5.54 us (3%)
  local copies, waits for them, and re-layouts  5.11 us (3%)
    pallas_call x1, Pallas kernels, send_units(): pl.pallas_call(functools.partial(send_kernel, 'sp', n), out_shape=[jax.Sh...  42 us
    pallas_call x1, Pallas kernels, summed_weight(): pl.pallas_call(functools.partial(weight_kernel, 'sp', n), out_shape=jax.S...  38.3 us
    pallas_call x1, Pallas kernels, exchange(): pl.pallas_call(functools.partial(exchange_kernel, axis, n, parts), out_sh...  33.9 us
    pallas_call x1, Pallas kernels, attention(): pl.pallas_call(functools.partial(attention_kernel, block), out_shape=jax....  22.2 us
    unnamed x3, local copies, waits for them, and re-layouts  3.41 us
  transfers between devices with their start and end apart: 1, of which 0 were waited for; matrix products, arithmetic and copies ran while one was open for 0% of the time, Pallas kernels for 23%

profile of v1, /device:TPU:0, one launch (start us, length us, event | category | flops | bytes accessed | tf_op | source)
XLA Modules:
  0.0 163.9 jit_solution(11001234912498826628)
XLA Ops:
  7.2 0.0 copy-start
  7.2 0.0 reduce-scatter.2.cloned.1.call-start
  7.2 1.5 copy-done
  8.8 2.8 %convolution_convert_fusion.1.v_ref = bf16[288,512]{1,0:T(8,128)(2,1)} fusion(bf16[288,2048]{1,0:T(8,128)(2,1)} %lat_ref.1, bf16[2048,512]{1,0:T(8,128)(2,1)S(1)} %copy-done), kind=kOutput, calls=%fused_computation.1 | convolution fusion | flops 604127232 | bytes 3571712 | tf_op jit(solution)/shard_map/dot_general | solution.py:507
  11.5 42.0 %shard_map.120 = (bf16[8,288,384]{2,1,0:T(8,128)(2,1)}, f32[8,8,288]{2,1,0:T(8,128)}) custom-call(bf16[288,512]{1,0:T(8,128)(2,1)} %q_ref.1, bf16[288,512]{1,0:T(8,128)(2,1)} %k_ref.1, bf16[288,512]{1,0:T(8,128)(2,1)} %convolution_convert_fusion.1.v_ref, bf16[288,512]{1,0:T(8,128)(2,1)} %first_ref.1, bf16[288,512]{1,0:T(8,128)(2,1)} %second_ref.1, ...), custom_call_target="tpu_custom_call" | custom-call | bytes 9437184 | tf_op jit(solution)/shard_map/pallas_call | solution.py:268
  53.5 0.9 copy.13
  54.4 0.1 reshape.18
  54.5 0.7 copy.16
  55.2 22.2 %shard_map.121 = bf16[2304,256]{1,0:T(8,128)(2,1)} custom-call(bf16[2304,384]{1,0:T(8,128)(2,1)} %bitcast.15, f32[9,8,256]{2,1,0:T(8,128)} %bitcast.13), custom_call_target="tpu_custom_call" | custom-call | flops 2642411520 | bytes 3686400 | tf_op jit(solution)/shard_map/pallas_call | solution.py:380
  77.4 33.9 %shard_map.122.x_ref = bf16[8,288,256]{2,1,0:T(8,128)(2,1)} custom-call(bf16[8,288,256]{2,1,0:T(8,128)(2,1)} %bitcast.11), custom_call_target="tpu_custom_call" | custom-call | bytes 18874368 | tf_op jit(solution)/shard_map/pallas_call | solution.py:206
  111.3 2.7 %shard_map.123 = (f32[288,512]{1,0:T(8,128)}, f32[288,512]{1,0:T(8,128)}, bf16[288,512]{1,0:T(8,128)(2,1)}) custom-call(bf16[8,288,256]{2,1,0:T(8,128)(2,1)} %shard_map.122.x_ref, f32[4]{0:T(128)} %lambda_ref.3), custom_call_target="tpu_custom_call" | custom-call | bytes 3538944 | tf_op jit(solution)/shard_map/pallas_call | solution.py:303
  114.0 2.8 %convolution_convert_fusion = bf16[288,2048]{1,0:T(8,128)(2,1)} fusion(bf16[288,512]{1,0:T(8,128)(2,1)} %get-tuple-element.13.dv_ref, bf16[2048,512]{1,0:T(8,128)(2,1)S(1)} %copy-done), kind=kOutput, calls=%fused_computation | convolution fusion | flops 604569600 | bytes 3571712 | tf_op jit(solution)/shard_map/dot_general | solution.py:516
  116.8 0.0 reduce-scatter.2.cloned.1.call-update
  116.8 38.3 %shard_map.124 = f32[256,512]{1,0:T(8,128)} custom-call(bf16[288,2048]{1,0:T(8,128)(2,1)} %lat_ref.1, bf16[288,512]{1,0:T(8,128)(2,1)} %get-tuple-element.13.dv_ref), custom_call_target="tpu_custom_call" | custom-call | flops 603979776 | bytes 67108864 | tf_op jit(solution)/shard_map/pallas_call | solution.py:479
  155.1 0.0 reduce-scatter.2.cloned.1.call-done
  155.2 1.9 %copy.18 = f32[256,512]{1,0:T(8,128)} copy(f32[256,512]{1,0:T(8,128)} %shard_map.124) | data formatting | bytes 1048576
Async XLA Ops:
  7.2 1.6 copy-start
  7.2 148.0 %reduce-scatter.2.cloned.1.call-start = ((), (), s32[]{:S(2)}) async-start(), calls=%async_computation.1 | async-start | bytes 1474560 | tf_op jit(solution)/shard_map/reduce_scatter | solution.py:519
Sparse Core Ops, SparseCore 0:
  117.0 29.0 reduce-scatter.1
